TPU v7x, 1024 devices: a whole 4x4x32 slice. The times are simulated.
1024 devices in a mesh: sp: 128 (over z, y), tp: 8 (over x, core).
Axes of the slice: x: 4, y: 4, z: 32, core: 2. Of those that a mesh axis runs over, the one named last changes fastest.
Arguments:
- latent: bfloat16 [16384, 2048], P(('sp', 'tp')), may hold values from -6 to 6
- context: bfloat16 [512, 2048], replicated, may hold values from -6 to 6
- condition: float32 [2048], replicated, may hold values from -6 to 6
- context_condition: float32 [2048], replicated, may hold values from -6 to 6
- modulation_weight: bfloat16 [2048, 3, 2048], P('sp', None, 'tp'), may hold values from -0.75 to 0.75
- norm_gain: float32 [2048], replicated, may hold values from 0.1 to 1.9
- gate_weight: bfloat16 [2048, 1024], P(None, 'tp'), may hold values from -0.125 to 0.125
- value_weight: bfloat16 [2048, 1024], P(None, 'tp'), may hold values from -0.125 to 0.125
- write_weight: bfloat16 [2048, 512], P(None, 'tp'), may hold values from -0.125 to 0.125
- read_weight: bfloat16 [2048, 512], P(None, 'tp'), may hold values from -0.125 to 0.125
- step_weight: bfloat16 [2048, 2, 16], replicated, may hold values from -0.125 to 0.125
- value_taps: bfloat16 [3, 1024], P(None, 'tp'), may hold values from -3.5 to 3.5
- map_taps: bfloat16 [3, 2, 512], P(None, None, 'tp'), may hold values from -3.5 to 3.5
- decay_rate: float32 [2, 16], replicated, may hold values from 1e-06 to 0.06
- decay_jump: float32 [2, 16, 16384], P(None, 'tp', 'sp'), may hold values from -2.76 to 0
- skip_gain: float32 [16], replicated, may hold values from 1 to 16
- group_gain: float32 [1024], P('tp'), may hold values from 0.1 to 1.9
- output_weight: bfloat16 [1024, 2048], P('tp'), may hold values from -0.1875 to 0.1875
- post_gain: float32 [2048], replicated, may hold values from 0.1 to 1.9
Outputs:
- updated: bfloat16 [16384, 2048], P(('sp', 'tp'))
All inputs are finite; a program needn't handle non-finite values.
Results may differ from a plain program's by a relative error of at most 0.014.
Values may be sent and summed in bfloat16 or wider, within the bound.
A program may use at most 64 MiB of HBM per device.

v0:
```python
import jax
import jax.numpy as jnp
from jax import lax
from jax.experimental import pallas as pl
from jax.experimental.pallas import tpu as pltpu
from jax.sharding import Mesh
from jax.sharding import PartitionSpec as P

SP = ("za", "zb", "y")
SP_TP = ("za", "zb", "y", "tp")
MESH = pl.DeviceIdType.MESH
EPSILON = 1e-06
HIGHEST = lax.Precision.HIGHEST
F32 = jnp.float32
BF16 = jnp.bfloat16
NA, NB, NY, NT = 8, 4, 4, 8
NI = NB * NY
NS = NA * NI
D = 2048
ROWS = 16
RANGE = 128
CTX = 512


def silu(x):
    return x * (1.0 / (1.0 + jnp.exp(-x)))


def softplus(x):
    return jnp.maximum(x, 0.0) + jnp.log1p(jnp.exp(-jnp.abs(x)))


def dot_f32(x, y):
    return jnp.dot(x, y, precision=HIGHEST, preferred_element_type=F32)


def dot_bf16(x, y):
    return jnp.dot(x.astype(BF16), y.astype(BF16), preferred_element_type=F32)


def iota(shape, dim):
    return lax.broadcasted_iota(jnp.int32, shape, dim)


def kernel(
    latent,
    cond,
    ccond,
    modw,
    ngain,
    vtaps,
    mtaps,
    rate,
    jump,
    skip,
    ggain,
    pgain,
    context_h,
    gate_h,
    value_h,
    write_h,
    read_h,
    step_h,
    outw_h,
    out,
    context_v,
    write_v,
    read_v,
    step_v,
    outw_v,
    wall,
    part,
    r1,
    s1,
    r2,
    r3,
    r4,
    xg,
    xn,
    cn,
    hid,
    hctx,
    uctx,
    lsend,
    rl1,
    l2send,
    rl2,
    sp,
    rs1,
    bt,
    rs2,
    cpre,
    ppre,
    cst,
    osend,
    rs3,
    oo,
    ro,
    load_sem,
    near_ssem,
    near_rsem,
    far_ssem,
    far_rsem,
    tp_ssem,
    tp_rsem,
    y_ssem,
    y_rsem,
    halo_ssem,
    halo_rsem,
):
    a = lax.axis_index("za")
    b = lax.axis_index("zb")
    y = lax.axis_index("y")
    t = lax.axis_index("tp")
    i = b * NY + y
    s = a * NI + i
    direction = lax.div(i, 8)

    def near(j):
        return {"zb": lax.div(j, NY), "y": lax.rem(j, NY)}

    def far(j):
        return {"za": j}

    def along_y(j):
        return {"y": j}

    def along_tp(j):
        return {"tp": j}

    def at_range(n):
        return {"za": lax.div(n, NI), "zb": lax.div(lax.rem(n, NI), NY), "y": lax.rem(n, NY)}

    following = at_range(lax.rem(s + 1, NS))
    preceding = at_range(lax.rem(s + NS - 1, NS))

    def copy(src, dst, ssem, rsem, device):
        return pltpu.make_async_remote_copy(
            src_ref=src, dst_ref=dst, send_sem=ssem, recv_sem=rsem, device_id=device, device_id_type=MESH
        )

    def exchange(n, me, peer, src_of, dst, ssem, rsem):
        def begin(k, carry):
            j = lax.rem(me + k, n)
            copy(src_of(j), dst.at[me], ssem.at[k], rsem.at[me], peer(j)).start()
            return carry

        def arrive(k, carry):
            j = lax.rem(me + n - k, n)
            copy(src_of(j), dst.at[j], ssem.at[k], rsem.at[j], peer(j)).wait_recv()
            return carry

        def leave(k, carry):
            j = lax.rem(me + k, n)
            copy(src_of(j), dst.at[me], ssem.at[k], rsem.at[me], peer(j)).wait_send()
            return carry

        return (
            lambda: lax.fori_loop(1, n, begin, 0),
            lambda: lax.fori_loop(1, n, arrive, 0),
            lambda: lax.fori_loop(1, n, leave, 0),
        )

    barrier = pltpu.get_barrier_semaphore()

    def tell(device):
        pl.semaphore_signal(barrier, inc=1, device_id=device, device_id_type=MESH)

    def tell_all(n, me, peer):
        def one(k, carry):
            tell(peer(lax.rem(me + k, n)))
            return carry

        lax.fori_loop(1, n, one, 0)

    tell_all(NA, a, far)
    tell_all(NI, i, near)
    tell_all(NT, t, along_tp)
    tell(following)
    tell(preceding)

    loads = [
        pltpu.make_async_copy(gate_h, wall.at[:, pl.ds(0, 128)], load_sem.at[0]),
        pltpu.make_async_copy(value_h, wall.at[:, pl.ds(128, 128)], load_sem.at[1]),
        pltpu.make_async_copy(write_h, write_v, load_sem.at[2]),
        pltpu.make_async_copy(read_h, read_v, load_sem.at[3]),
        pltpu.make_async_copy(step_h, step_v, load_sem.at[4]),
        pltpu.make_async_copy(context_h, context_v, load_sem.at[5]),
        pltpu.make_async_copy(outw_h, outw_v, load_sem.at[6]),
    ]
    for load in loads:
        load.start()

    lane = iota((1, 128), 1)
    mine = lax.div(lane, ROWS) == lax.rem(s, 8)
    rows8 = iota((8, 128), 0)
    first = jnp.where(mine, silu(cond[pl.ds(lax.div(s, 8), 1), :]), 0.0)
    second = jnp.where(mine, silu(ccond[pl.ds(lax.div(s, 8), 1), :]), 0.0)
    both = jnp.where(rows8 == 0, first, jnp.where(rows8 == 1, second, 0.0))
    weight = modw[...].astype(F32)
    pieces = dot_f32(both, jnp.concatenate([weight] * 8, axis=0))
    for m in range(12):
        r, k, half = m // 6, (m % 6) // 2, m % 2
        low = k * 256 + half * 128
        part[m // 3, m % 3 : m % 3 + 1, :] = pieces[r : r + 1, low : low + 128]

    m1_start, m1_wait, m1_left = exchange(
        NI, i, near, lambda j: part.at[lax.rem(j, NY)], r1, near_ssem.at[0], near_rsem.at[0]
    )
    m2_start, m2_wait, m2_left = exchange(NA, a, far, lambda j: s1, r2, far_ssem.at[0], far_rsem.at[0])
    m3_start, m3_wait, m3_left = exchange(NY, y, along_y, lambda j: r3.at[y], r3, y_ssem, y_rsem)
    m4_start, m4_wait, m4_left = exchange(NT, t, along_tp, lambda j: r3, r4, tp_ssem.at[1], tp_rsem.at[1])
    x_start, x_wait, x_left = exchange(NT, t, along_tp, lambda j: latent, xg, tp_ssem.at[0], tp_rsem.at[0])

    pl.semaphore_wait(barrier, (NA - 1) + (NI - 1) + (NT - 1) + 2)

    m1_start()
    r1[i] = part[y]
    x_start()
    xg[t] = latent[...]

    for load in loads[:5]:
        load.wait()

    def join(k, carry):
        at = pl.ds(pl.multiple_of(k * 256, 256), 256)
        wall[at, 256:384] = jnp.concatenate([write_v[at, :], read_v[at, :]], axis=1)
        wall[at, 384:512] = jnp.concatenate([step_v[at, :], jnp.zeros((256, 96), BF16)], axis=1)
        return carry

    lax.fori_loop(0, D // 256, join, 0)

    m1_wait()
    s1[...] = jnp.sum(r1[...], axis=0)
    m2_start()
    r2[a] = s1[...]

    x_wait()
    up = copy(xg.at[NT - 1], xg.at[NT], halo_ssem.at[0], halo_rsem.at[0], following)
    down = copy(xg.at[0], xg.at[NT + 1], halo_ssem.at[1], halo_rsem.at[1], preceding)
    up.start()
    down.start()
    gain = ngain[...]

    def normed(x):
        return x * lax.rsqrt(jnp.mean(x * x, axis=-1, keepdims=True) + EPSILON) * gain

    def norm_latent(k, carry):
        xn[k] = normed(xg[k].astype(F32))
        return carry

    lax.fori_loop(0, NT, norm_latent, 0)
    up.wait_recv()
    down.wait_recv()
    lax.fori_loop(NT, NT + 2, norm_latent, 0)
    loads[5].wait()

    def norm_context(k, carry):
        at = pl.ds(pl.multiple_of(k * 16, 16), 16)
        cn[at, :] = normed(context_v[at, :].astype(F32))
        return carry

    lax.fori_loop(0, CTX // 16, norm_context, 0)

    m2_wait()
    r3[y] = jnp.sum(r2[...], axis=0)
    m3_start()
    m3_wait()
    m4_start()
    r4[t] = r3[...]
    m4_wait()

    def vector(r, k):
        found = []
        for j in range(NT):
            for half in range(2):
                m = (r * 3 + k) * 2 + half
                found.append(r4[j, m // 3, m % 3 : m % 3 + 1, :])
        return jnp.concatenate(found, axis=1)

    shift0, scale0 = vector(0, 0), 1.0 + vector(0, 1)

    def modulate(k, carry):
        hid[pl.ds(pl.multiple_of(k * 16, 16), 16), :] = (xn[k] * scale0 + shift0).astype(BF16)
        return carry

    lax.fori_loop(0, NT + 2, modulate, 0)
    linear = jnp.dot(hid[...], wall[...], preferred_element_type=F32).astype(BF16).astype(F32)
    gate_linear = linear[:RANGE, :128]
    u = linear[:RANGE, 128:384]
    step_linear = linear[:RANGE, 384:512]
    before = jnp.where(s > 0, linear[RANGE + 15 : RANGE + 16, 128:384], 0.0)
    after = jnp.where(s < NS - 1, linear[RANGE + 16 : RANGE + 17, 128:384], 0.0)
    vt = vtaps[...].astype(F32)

    def taps(k):
        m = mtaps[k].astype(F32)
        return jnp.concatenate([vt[k : k + 1, :], m[0:1, :], m[1:2, :]], axis=1)

    tap = [taps(k) for k in range(3)]

    def conv(u, before, after):
        n = u.shape[0]
        row = iota(u.shape, 0)
        lower = jnp.where(row == 0, before, pltpu.roll(u, 1, 0))
        upper = jnp.where(row == n - 1, after, pltpu.roll(u, n - 1, 0))
        return silu(tap[0] * lower + tap[1] * u + tap[2] * upper)

    k8 = iota((8, 128), 0)
    lane8 = iota((8, 128), 1)
    chosen = jnp.where((k8 < 4) & (lane8 == lax.div(k8, 2) * 16 + 2 * t + lax.rem(k8, 2)), 1.0, 0.0)

    def own_steps(step_linear):
        return softplus(
            lax.dot_general(
                chosen.astype(BF16),
                step_linear.astype(BF16),
                (((1,), (1,)), ((), ())),
                preferred_element_type=F32,
            )
        )

    rates = jnp.zeros((8, 128), F32)
    for k in range(4):
        rates = jnp.where(k8 == k, rate[k // 2, 2 * t + k % 2], rates)
    jumps = jnp.concatenate([jump[0], jump[1], jnp.zeros((4, 128), F32)], axis=0)
    size_row = own_steps(step_linear)
    decay_row = jumps - size_row * rates
    ri = iota((128, 128), 0)
    ci = iota((128, 128), 1)
    upto = jnp.where(ri <= ci, 1.0, 0.0)
    onwards = jnp.where(ri >= ci, 1.0, 0.0)
    within_row = jnp.where(k8 < 2, dot_f32(decay_row, upto), dot_f32(decay_row, onwards))
    total = jnp.sum(decay_row, axis=1, keepdims=True)
    low_lanes = lane < 64

    def total_lanes(d):
        return jnp.where(low_lanes, total[2 * d : 2 * d + 1, :], total[2 * d + 1 : 2 * d + 2, :])

    lsend[0:1, :] = total_lanes(0)
    lsend[1:2, :] = total_lanes(1)
    l1_start, l1_wait, l1_left = exchange(NI, i, near, lambda j: lsend, rl1, near_ssem.at[1], near_rsem.at[1])
    l1_start()
    rl1[i] = lsend[...]

    columns = jnp.concatenate(
        [within_row, jnp.exp(total - within_row) * size_row, jnp.exp(within_row), jnp.zeros((104, 128), F32)],
        axis=0,
    ).T

    def head_columns(columns, base, d):
        at = base + 2 * d
        return jnp.where(low_lanes, columns[:, at : at + 1], columns[:, at + 1 : at + 2])

    mixed = conv(u, before, after)
    values = mixed[:, :128]
    writes = mixed[:, 128:192].astype(BF16)
    reads = mixed[:, 192:256].astype(BF16)

    def state_of(writes, weighted):
        return lax.dot_general(
            writes.astype(BF16),
            weighted.astype(BF16),
            (((0,), (0,)), ((), ())),
            preferred_element_type=F32,
        )

    for d in range(2):
        sp[8 * d : 8 * d + 8] = state_of(writes, values * head_columns(columns, 8, d)).reshape(8, 8, 128)
    s1_start, s1_wait, s1_left = exchange(NI, i, near, lambda j: sp.at[j], rs1, near_ssem.at[2], near_rsem.at[2])
    s1_start()
    rs1[i] = sp[i]

    scores = lax.dot_general(reads, writes, (((1,), (1,)), ((), ())), preferred_element_type=F32)
    inner = []
    for h in range(2):
        fading = jnp.zeros((128, 128), F32)
        for d in range(2):
            k = 2 * d + h
            gap = columns[:, k : k + 1] - within_row[k : k + 1, :]
            mask = (ri >= ci) if d == 0 else (ri <= ci)
            fading = fading + jnp.exp(jnp.where(mask, gap, -1e30)) * size_row[k : k + 1, :]
        inner.append(dot_bf16(scores * fading, values[:, 64 * h : 64 * h + 64]))
    skips = jnp.where(low_lanes, skip[2 * t], skip[2 * t + 1])
    local = skips * values + jnp.concatenate(inner, axis=1)
    gates = silu(gate_linear)

    l1_wait()
    l2send[...] = jnp.sum(rl1[...], axis=0)
    l2_start, l2_wait, l2_left = exchange(NA, a, far, lambda j: l2send, rl2, far_ssem.at[1], far_rsem.at[1])
    l2_start()
    rl2[a] = l2send[...]

    s1_wait()

    def fold(k, carry):
        state, product = carry
        j = k + direction * (NI - 1 - 2 * k)
        cpre[j] = state
        ppre[j] = product
        logs = rl1[j]
        factor = jnp.exp(jnp.where(direction == 0, logs[0:1, :], logs[1:2, :]))
        return factor * state + rs1[j], factor * product

    block_state, _ = lax.fori_loop(
        0, NI, fold, (jnp.zeros((8, 128), F32), jnp.ones((1, 128), F32))
    )
    bt[...] = block_state
    s2_start, s2_wait, s2_left = exchange(NA, a, far, lambda j: bt, rs2, far_ssem.at[2], far_rsem.at[2])
    s2_start()
    rs2[a] = bt[...]

    shift1, scale1 = vector(1, 0), 1.0 + vector(1, 1)

    def context_chunk(k, carry):
        def mod(m, carry):
            at = pl.ds(pl.multiple_of(k * 128 + m * 16, 16), 16)
            hctx[pl.ds(pl.multiple_of(m * 16, 16), 16), :] = (cn[at, :] * scale1 + shift1).astype(BF16)
            return carry

        lax.fori_loop(0, 8, mod, 0)
        found = jnp.dot(hctx[...], wall[:, 128:512], preferred_element_type=F32)
        uctx[pl.ds(pl.multiple_of(k * 128, 128), 128), :] = found.astype(BF16).astype(F32)
        return carry

    lax.fori_loop(0, CTX // 128, context_chunk, 0)
    context_mixed = conv(uctx[:, :256], jnp.zeros((1, 256), F32), jnp.zeros((1, 256), F32))
    context_values = context_mixed[:, :128]
    context_writes = context_mixed[:, 128:192]
    chunks = CTX // 128
    c_size = [own_steps(uctx[128 * c : 128 * c + 128, 256:384]) for c in range(chunks)]
    c_decay = [-size * rates for size in c_size]
    c_total = [jnp.sum(decay, axis=1, keepdims=True) for decay in c_decay]
    later = jnp.where(ri > ci, 1.0, 0.0)
    earlier = jnp.where(ri < ci, 1.0, 0.0)
    context_state = [jnp.zeros((64, 128), F32), jnp.zeros((64, 128), F32)]
    for c in range(chunks):
        after_it = sum(c_total[c + 1 :], jnp.zeros((8, 1), F32))
        before_it = sum(c_total[:c], jnp.zeros((8, 1), F32))
        rest = jnp.where(
            k8 < 2, dot_f32(c_decay[c], later) + after_it, dot_f32(c_decay[c], earlier) + before_it
        )
        turned = jnp.concatenate([jnp.exp(rest) * c_size[c], jnp.zeros((120, 128), F32)], axis=0).T
        at = slice(128 * c, 128 * c + 128)
        for d in range(2):
            context_state[d] = context_state[d] + state_of(
                context_writes[at], context_values[at] * head_columns(turned, 0, d)
            )
    for d in range(2):
        cst[8 * d : 8 * d + 8] = context_state[d].reshape(8, 8, 128)

    l2_wait()
    s2_wait()
    place = a + direction * (NA - 1 - 2 * a)

    def enter(k, state):
        j = k + direction * (NA - 1 - 2 * k)
        logs = rl2[j]
        factor = jnp.exp(jnp.where(direction == 0, logs[0:1, :], logs[1:2, :]))
        return jnp.where(k < place, factor * state + rs2[j], state)

    entering = lax.fori_loop(0, NA, enter, cst[i])

    def hand_out(k, carry):
        osend[k] = cpre[k] + ppre[k] * entering
        return carry

    lax.fori_loop(0, NI, hand_out, 0)
    s3_start, s3_wait, s3_left = exchange(NI, i, near, lambda j: osend.at[j], rs3, near_ssem.at[3], near_rsem.at[3])
    s3_start()
    rs3[i] = osend[i]
    s3_wait()

    mixer = local
    for d in range(2):
        came = rs3[8 * d : 8 * d + 8].reshape(64, 128)
        mixer = mixer + dot_bf16(reads, came) * head_columns(columns, 16, d)
    gated = mixer * gates
    gated = gated * lax.rsqrt(jnp.mean(gated * gated, axis=-1, keepdims=True) + EPSILON) * ggain[...]
    gated = gated.astype(BF16)
    loads[6].wait()
    for n in range(4):
        at = slice(512 * n, 512 * n + 512)
        oo[:, :, at] = (
            jnp.dot(gated, outw_v[:, at], preferred_element_type=F32).astype(BF16).reshape(NT, ROWS, 512)
        )
    o_start, o_wait, o_left = exchange(NT, t, along_tp, lambda j: oo.at[j], ro, tp_ssem.at[2], tp_rsem.at[2])
    o_start()
    ro[t] = oo[t]
    gate0 = vector(0, 2)
    o_wait()
    summed = ro[0].astype(F32)
    for j in range(1, NT):
        summed = summed + ro[j].astype(F32)
    normed_out = (
        summed * lax.rsqrt(jnp.mean(summed * summed, axis=-1, keepdims=True) + EPSILON) * pgain[...]
    )
    out[...] = (latent[...].astype(F32) + gate0 * normed_out).astype(BF16)

    for left in (m1_left, m2_left, m3_left, m4_left, x_left, l1_left, l2_left, s1_left, s2_left, s3_left, o_left):
        left()
    up.wait_send()
    down.wait_send()


def body(
    latent,
    context,
    condition,
    context_condition,
    modulation_weight,
    norm_gain,
    gate_weight,
    value_weight,
    write_weight,
    read_weight,
    step_weight,
    value_taps,
    map_taps,
    decay_rate,
    decay_jump,
    skip_gain,
    group_gain,
    output_weight,
    post_gain,
):
    vmem = pl.BlockSpec(memory_space=pltpu.VMEM)
    smem = pl.BlockSpec(memory_space=pltpu.SMEM)
    hbm = pl.BlockSpec(memory_space=pl.ANY)
    dma = pltpu.SemaphoreType.DMA
    return pl.pallas_call(
        kernel,
        out_shape=jax.ShapeDtypeStruct((ROWS, D), BF16),
        in_specs=[vmem, vmem, vmem, vmem, vmem, vmem, vmem, smem, vmem, smem, vmem, vmem] + [hbm] * 7,
        out_specs=vmem,
        scratch_shapes=[
            pltpu.VMEM((CTX, D), BF16),
            pltpu.VMEM((D, 64), BF16),
            pltpu.VMEM((D, 64), BF16),
            pltpu.VMEM((D, 32), BF16),
            pltpu.VMEM((128, D), BF16),
            pltpu.VMEM((D, 512), BF16),
            pltpu.VMEM((NY, 4, 128), F32),
            pltpu.VMEM((NI, 4, 128), F32),
            pltpu.VMEM((4, 128), F32),
            pltpu.VMEM((NA, 4, 128), F32),
            pltpu.VMEM((NY, 4, 128), F32),
            pltpu.VMEM((NT, NY, 4, 128), F32),
            pltpu.VMEM((NT + 2, ROWS, D), BF16),
            pltpu.VMEM((NT + 2, ROWS, D), F32),
            pltpu.VMEM((CTX, D), F32),
            pltpu.VMEM(((NT + 2) * ROWS, D), BF16),
            pltpu.VMEM((128, D), BF16),
            pltpu.VMEM((CTX, 384), F32),
            pltpu.VMEM((2, 128), F32),
            pltpu.VMEM((NI, 2, 128), F32),
            pltpu.VMEM((2, 128), F32),
            pltpu.VMEM((NA, 2, 128), F32),
            pltpu.VMEM((NI, 8, 128), F32),
            pltpu.VMEM((NI, 8, 128), F32),
            pltpu.VMEM((8, 128), F32),
            pltpu.VMEM((NA, 8, 128), F32),
            pltpu.VMEM((NI, 8, 128), F32),
            pltpu.VMEM((NI, 1, 128), F32),
            pltpu.VMEM((NI, 8, 128), F32),
            pltpu.VMEM((NI, 8, 128), F32),
            pltpu.VMEM((NI, 8, 128), F32),
            pltpu.VMEM((NT, ROWS, D), BF16),
            pltpu.VMEM((NT, ROWS, D), BF16),
            dma((7,)),
            dma((4, NI)),
            dma((4, NI)),
            dma((3, NA)),
            dma((3, NA)),
            dma((3, NT)),
            dma((3, NT)),
            dma((NY,)),
            dma((NY,)),
            dma((2,)),
            dma((2,)),
        ],
        compiler_params=pltpu.CompilerParams(
            collective_id=0, has_side_effects=True, vmem_limit_bytes=60 * 1024 * 1024
        ),
    )(
        latent,
        condition.reshape(16, 128),
        context_condition.reshape(16, 128),
        modulation_weight.reshape(ROWS, 768),
        norm_gain.reshape(1, D),
        value_taps,
        map_taps,
        decay_rate,
        decay_jump,
        skip_gain,
        group_gain.reshape(1, 128),
        post_gain.reshape(1, D),
        context,
        gate_weight,
        value_weight,
        write_weight,
        read_weight,
        step_weight.reshape(D, 32),
        output_weight,
    )


def solution(mesh):
    torus = Mesh(mesh.devices.reshape(NA, NB, NY, NT), SP_TP)
    return jax.shard_map(
        body,
        mesh=torus,
        in_specs=(
            P(SP_TP, None),
            P(),
            P(),
            P(),
            P(SP, None, "tp"),
            P(),
            P(None, "tp"),
            P(None, "tp"),
            P(None, "tp"),
            P(None, "tp"),
            P(),
            P(None, "tp"),
            P(None, None, "tp"),
            P(),
            P(None, "tp", SP),
            P(),
            P("tp"),
            P("tp", None),
            P(),
        ),
        out_specs=P(SP_TP, None),
        check_vma=False,
    )
```

profile of v0, /device:TPU:1, one launch (start us, length us, event | category | flops | bytes accessed | tf_op | source)
XLA Modules:
  0.0 97.8 jit_solution(18147163110299376616)
XLA Ops:
  0.0 1.3 %copy.28 = bf16[3,2,8,256]{3,2,0,1:T(8,128)(2,1)} copy(bf16[3,2,8,256]{3,2,1,0:T(8,128)(2,1)} %bitcast.10) | data formatting | bytes 49152 | tf_op jit(solution)/shard_map/reshape | solution.py:589
  1.3 1.9 %copy.25.write_h = bf16[2048,64]{1,0:T(8,128)(2,1)} copy(bf16[2048,64]{0,1:T(8,128)(2,1)} %param.27) | data formatting | bytes 524288 | tf_op args[8]
  3.3 2.0 %copy.26.read_h = bf16[2048,64]{1,0:T(8,128)(2,1)} copy(bf16[2048,64]{0,1:T(8,128)(2,1)} %param.28) | data formatting | bytes 524288 | tf_op args[9]
  5.3 1.9 %copy.27.step_h = bf16[2048,32]{1,0:T(8,128)(2,1)} copy(bf16[2048,32]{0,1:T(8,128)(2,1)} %bitcast.8) | data formatting | bytes 262144 | tf_op jit(solution)/shard_map/reshape | solution.py:603
  7.2 89.1 %shard_map.181 = bf16[16,2048]{1,0:T(8,128)(2,1)} custom-call(bf16[16,2048]{1,0:T(8,128)(2,1)} %latent.1, f32[16,128]{1,0:T(8,128)} %bitcast.11, f32[16,128]{1,0:T(8,128)} %bitcast.12, bf16[16,768]{1,0:T(8,128)(2,1)} %bitcast.9, f32[1,2048]{1,0:T(1,128)} %bitcast.13, bf16[3,128]{1,0:T(4,128)(2,1)} %vtaps.1, bf16[3,2,64]{2,1,0:T(2,128)(2,1)} %mtaps.1, ...), custom_call_target="tpu_custom_call" | custom-call | tf_op jit(solution)/shard_map/pallas_call | solution.py:531
  96.3 1.5 %copy.30 = bf16[16,2048]{1,0:T(8,128)(2,1)} copy(bf16[16,2048]{1,0:T(8,128)(2,1)} %shard_map.181) | data formatting | bytes 131072
where the time goes:
time: 98.1 us; the launch traced here: 97.8 us
  Pallas kernels  89.1 us (91%)
  local copies, waits for them, and re-layouts  8.67 us (9%)
    pallas_call x1, Pallas kernels, body(): pl.pallas_call(kernel, out_shape=jax.ShapeDtypeStruct((ROWS, D), BF16), i...  89.1 us
    unnamed x3, local copies, waits for them, and re-layouts  5.39 us

commit v1 on v0

--- a/solution.py
+++ b/solution.py
@@ -43,6 +43,26 @@
 
 
 def kernel(
+    latent_h,
+    cond_h,
+    ccond_h,
+    modw_h,
+    ngain_h,
+    vtaps_h,
+    mtaps_h,
+    rate_h,
+    jump_h,
+    skip_h,
+    ggain_h,
+    pgain_h,
+    context_h,
+    gate_h,
+    value_h,
+    write_h,
+    read_h,
+    step_h,
+    outw_h,
+    out,
     latent,
     cond,
     ccond,
@@ -55,27 +75,19 @@
     skip,
     ggain,
     pgain,
-    context_h,
-    gate_h,
-    value_h,
-    write_h,
-    read_h,
-    step_h,
-    outw_h,
-    out,
     context_v,
-    write_v,
-    read_v,
-    step_v,
+    rest_v,
     outw_v,
     wall,
     part,
     r1,
     s1,
     r2,
-    r3,
+    s2,
     r4,
     xg,
+    hsend,
+    hrecv,
     xn,
     cn,
     hid,
@@ -96,6 +108,7 @@
     rs3,
     oo,
     ro,
+    small_sem,
     load_sem,
     near_ssem,
     near_rsem,
@@ -103,8 +116,8 @@
     far_rsem,
     tp_ssem,
     tp_rsem,
-    y_ssem,
-    y_rsem,
+    plane_ssem,
+    plane_rsem,
     halo_ssem,
     halo_rsem,
 ):
@@ -114,6 +127,7 @@
     t = lax.axis_index("tp")
     i = b * NY + y
     s = a * NI + i
+    g = y * NT + t
     direction = lax.div(i, 8)
 
     def near(j):
@@ -122,8 +136,8 @@
     def far(j):
         return {"za": j}
 
-    def along_y(j):
-        return {"y": j}
+    def plane(j):
+        return {"y": lax.div(j, NT), "tp": lax.rem(j, NT)}
 
     def along_tp(j):
         return {"tp": j}
@@ -175,21 +189,44 @@
 
     tell_all(NA, a, far)
     tell_all(NI, i, near)
-    tell_all(NT, t, along_tp)
+    tell_all(NY * NT, g, plane)
     tell(following)
     tell(preceding)
 
+    small = [
+        pltpu.make_async_copy(src, dst, small_sem.at[n])
+        for n, (src, dst) in enumerate(
+            (
+                (cond_h, cond),
+                (ccond_h, ccond),
+                (modw_h, modw),
+                (latent_h, latent),
+                (ngain_h, ngain),
+                (vtaps_h, vtaps),
+                (mtaps_h, mtaps),
+                (rate_h, rate),
+                (jump_h, jump),
+                (skip_h, skip),
+                (ggain_h, ggain),
+                (pgain_h, pgain),
+            )
+        )
+    ]
+    for load in small:
+        load.start()
     loads = [
         pltpu.make_async_copy(gate_h, wall.at[:, pl.ds(0, 128)], load_sem.at[0]),
         pltpu.make_async_copy(value_h, wall.at[:, pl.ds(128, 128)], load_sem.at[1]),
-        pltpu.make_async_copy(write_h, write_v, load_sem.at[2]),
-        pltpu.make_async_copy(read_h, read_v, load_sem.at[3]),
-        pltpu.make_async_copy(step_h, step_v, load_sem.at[4]),
+        pltpu.make_async_copy(write_h, rest_v.at[pl.ds(0, 64)], load_sem.at[2]),
+        pltpu.make_async_copy(read_h, rest_v.at[pl.ds(64, 64)], load_sem.at[3]),
+        pltpu.make_async_copy(step_h, rest_v.at[pl.ds(128, 32)], load_sem.at[4]),
         pltpu.make_async_copy(context_h, context_v, load_sem.at[5]),
         pltpu.make_async_copy(outw_h, outw_v, load_sem.at[6]),
     ]
     for load in loads:
         load.start()
+    for load in small:
+        load.wait()
 
     lane = iota((1, 128), 1)
     mine = lax.div(lane, ROWS) == lax.rem(s, 8)
@@ -197,7 +234,7 @@
     first = jnp.where(mine, silu(cond[pl.ds(lax.div(s, 8), 1), :]), 0.0)
     second = jnp.where(mine, silu(ccond[pl.ds(lax.div(s, 8), 1), :]), 0.0)
     both = jnp.where(rows8 == 0, first, jnp.where(rows8 == 1, second, 0.0))
-    weight = modw[...].astype(F32)
+    weight = jnp.concatenate([modw[k].astype(F32) for k in range(3)], axis=1)
     pieces = dot_f32(both, jnp.concatenate([weight] * 8, axis=0))
     for m in range(12):
         r, k, half = m // 6, (m % 6) // 2, m % 2
@@ -208,11 +245,10 @@
         NI, i, near, lambda j: part.at[lax.rem(j, NY)], r1, near_ssem.at[0], near_rsem.at[0]
     )
     m2_start, m2_wait, m2_left = exchange(NA, a, far, lambda j: s1, r2, far_ssem.at[0], far_rsem.at[0])
-    m3_start, m3_wait, m3_left = exchange(NY, y, along_y, lambda j: r3.at[y], r3, y_ssem, y_rsem)
-    m4_start, m4_wait, m4_left = exchange(NT, t, along_tp, lambda j: r3, r4, tp_ssem.at[1], tp_rsem.at[1])
+    m3_start, m3_wait, m3_left = exchange(NY * NT, g, plane, lambda j: s2, r4, plane_ssem, plane_rsem)
     x_start, x_wait, x_left = exchange(NT, t, along_tp, lambda j: latent, xg, tp_ssem.at[0], tp_rsem.at[0])
 
-    pl.semaphore_wait(barrier, (NA - 1) + (NI - 1) + (NT - 1) + 2)
+    pl.semaphore_wait(barrier, (NA - 1) + (NI - 1) + (NY * NT - 1) + 2)
 
     m1_start()
     r1[i] = part[y]
@@ -222,10 +258,11 @@
     for load in loads[:5]:
         load.wait()
 
+    rest_v[160:256, :] = jnp.zeros((96, D), BF16)
+
     def join(k, carry):
         at = pl.ds(pl.multiple_of(k * 256, 256), 256)
-        wall[at, 256:384] = jnp.concatenate([write_v[at, :], read_v[at, :]], axis=1)
-        wall[at, 384:512] = jnp.concatenate([step_v[at, :], jnp.zeros((256, 96), BF16)], axis=1)
+        wall[at, 256:512] = rest_v[:, at].T
         return carry
 
     lax.fori_loop(0, D // 256, join, 0)
@@ -236,8 +273,10 @@
     r2[a] = s1[...]
 
     x_wait()
-    up = copy(xg.at[NT - 1], xg.at[NT], halo_ssem.at[0], halo_rsem.at[0], following)
-    down = copy(xg.at[0], xg.at[NT + 1], halo_ssem.at[1], halo_rsem.at[1], preceding)
+    hsend[0] = xg[NT - 1].astype(F32)[15:16, :]
+    hsend[1] = xg[0].astype(F32)[0:1, :]
+    up = copy(hsend.at[0], hrecv.at[0], halo_ssem.at[0], halo_rsem.at[0], following)
+    down = copy(hsend.at[1], hrecv.at[1], halo_ssem.at[1], halo_rsem.at[1], preceding)
     up.start()
     down.start()
     gain = ngain[...]
@@ -252,7 +291,7 @@
     lax.fori_loop(0, NT, norm_latent, 0)
     up.wait_recv()
     down.wait_recv()
-    lax.fori_loop(NT, NT + 2, norm_latent, 0)
+    xn[NT] = jnp.concatenate([normed(hrecv[0]), normed(hrecv[1]), jnp.zeros((14, D), F32)], axis=0)
     loads[5].wait()
 
     def norm_context(k, carry):
@@ -263,19 +302,17 @@
     lax.fori_loop(0, CTX // 16, norm_context, 0)
 
     m2_wait()
-    r3[y] = jnp.sum(r2[...], axis=0)
+    s2[...] = jnp.sum(r2[...], axis=0)
     m3_start()
+    r4[g] = s2[...]
     m3_wait()
-    m4_start()
-    r4[t] = r3[...]
-    m4_wait()
 
     def vector(r, k):
         found = []
         for j in range(NT):
             for half in range(2):
                 m = (r * 3 + k) * 2 + half
-                found.append(r4[j, m // 3, m % 3 : m % 3 + 1, :])
+                found.append(r4[m // 3 * NT + j, m % 3 : m % 3 + 1, :])
         return jnp.concatenate(found, axis=1)
 
     shift0, scale0 = vector(0, 0), 1.0 + vector(0, 1)
@@ -284,13 +321,13 @@
         hid[pl.ds(pl.multiple_of(k * 16, 16), 16), :] = (xn[k] * scale0 + shift0).astype(BF16)
         return carry
 
-    lax.fori_loop(0, NT + 2, modulate, 0)
+    lax.fori_loop(0, NT + 1, modulate, 0)
     linear = jnp.dot(hid[...], wall[...], preferred_element_type=F32).astype(BF16).astype(F32)
     gate_linear = linear[:RANGE, :128]
     u = linear[:RANGE, 128:384]
     step_linear = linear[:RANGE, 384:512]
-    before = jnp.where(s > 0, linear[RANGE + 15 : RANGE + 16, 128:384], 0.0)
-    after = jnp.where(s < NS - 1, linear[RANGE + 16 : RANGE + 17, 128:384], 0.0)
+    before = jnp.where(s > 0, linear[RANGE : RANGE + 1, 128:384], 0.0)
+    after = jnp.where(s < NS - 1, linear[RANGE + 1 : RANGE + 2, 128:384], 0.0)
     vt = vtaps[...].astype(F32)
 
     def taps(k):
@@ -321,8 +358,13 @@
         )
 
     rates = jnp.zeros((8, 128), F32)
+    lane16 = iota((1, 16), 1)
+
+    def own(row, h):
+        return jnp.sum(jnp.where(lane16 == 2 * t + h, row, 0.0), axis=1, keepdims=True)
+
     for k in range(4):
-        rates = jnp.where(k8 == k, rate[k // 2, 2 * t + k % 2], rates)
+        rates = jnp.where(k8 == k, own(rate[k // 2 : k // 2 + 1, :], k % 2), rates)
     jumps = jnp.concatenate([jump[0], jump[1], jnp.zeros((4, 128), F32)], axis=0)
     size_row = own_steps(step_linear)
     decay_row = jumps - size_row * rates
@@ -366,7 +408,7 @@
         )
 
     for d in range(2):
-        sp[8 * d : 8 * d + 8] = state_of(writes, values * head_columns(columns, 8, d)).reshape(8, 8, 128)
+        sp[8 * d : 8 * d + 8] = state_of(writes, values * head_columns(columns, 8, d)).astype(BF16).reshape(8, 8, 128)
     s1_start, s1_wait, s1_left = exchange(NI, i, near, lambda j: sp.at[j], rs1, near_ssem.at[2], near_rsem.at[2])
     s1_start()
     rs1[i] = sp[i]
@@ -381,7 +423,7 @@
             mask = (ri >= ci) if d == 0 else (ri <= ci)
             fading = fading + jnp.exp(jnp.where(mask, gap, -1e30)) * size_row[k : k + 1, :]
         inner.append(dot_bf16(scores * fading, values[:, 64 * h : 64 * h + 64]))
-    skips = jnp.where(low_lanes, skip[2 * t], skip[2 * t + 1])
+    skips = jnp.where(low_lanes, own(skip[...], 0), own(skip[...], 1))
     local = skips * values + jnp.concatenate(inner, axis=1)
     gates = silu(gate_linear)
 
@@ -400,12 +442,12 @@
         ppre[j] = product
         logs = rl1[j]
         factor = jnp.exp(jnp.where(direction == 0, logs[0:1, :], logs[1:2, :]))
-        return factor * state + rs1[j], factor * product
+        return factor * state + rs1[j].astype(F32), factor * product
 
     block_state, _ = lax.fori_loop(
         0, NI, fold, (jnp.zeros((8, 128), F32), jnp.ones((1, 128), F32))
     )
-    bt[...] = block_state
+    bt[...] = block_state.astype(BF16)
     s2_start, s2_wait, s2_left = exchange(NA, a, far, lambda j: bt, rs2, far_ssem.at[2], far_rsem.at[2])
     s2_start()
     rs2[a] = bt[...]
@@ -449,6 +491,10 @@
     for d in range(2):
         cst[8 * d : 8 * d + 8] = context_state[d].reshape(8, 8, 128)
 
+    for left in (m1_left, m2_left, m3_left, x_left, l1_left, s1_left, l2_left, s2_left):
+        left()
+    up.wait_send()
+    down.wait_send()
     l2_wait()
     s2_wait()
     place = a + direction * (NA - 1 - 2 * a)
@@ -457,12 +503,12 @@
         j = k + direction * (NA - 1 - 2 * k)
         logs = rl2[j]
         factor = jnp.exp(jnp.where(direction == 0, logs[0:1, :], logs[1:2, :]))
-        return jnp.where(k < place, factor * state + rs2[j], state)
+        return jnp.where(k < place, factor * state + rs2[j].astype(F32), state)
 
     entering = lax.fori_loop(0, NA, enter, cst[i])
 
     def hand_out(k, carry):
-        osend[k] = cpre[k] + ppre[k] * entering
+        osend[k] = (cpre[k] + ppre[k] * entering).astype(BF16)
         return carry
 
     lax.fori_loop(0, NI, hand_out, 0)
@@ -497,10 +543,8 @@
     )
     out[...] = (latent[...].astype(F32) + gate0 * normed_out).astype(BF16)
 
-    for left in (m1_left, m2_left, m3_left, m4_left, x_left, l1_left, l2_left, s1_left, s2_left, s3_left, o_left):
-        left()
-    up.wait_send()
-    down.wait_send()
+    s3_left()
+    o_left()
 
 
 def body(
@@ -525,48 +569,60 @@
     post_gain,
 ):
     vmem = pl.BlockSpec(memory_space=pltpu.VMEM)
-    smem = pl.BlockSpec(memory_space=pltpu.SMEM)
     hbm = pl.BlockSpec(memory_space=pl.ANY)
     dma = pltpu.SemaphoreType.DMA
     return pl.pallas_call(
         kernel,
         out_shape=jax.ShapeDtypeStruct((ROWS, D), BF16),
-        in_specs=[vmem, vmem, vmem, vmem, vmem, vmem, vmem, smem, vmem, smem, vmem, vmem] + [hbm] * 7,
+        in_specs=[hbm] * 19,
         out_specs=vmem,
         scratch_shapes=[
+            pltpu.VMEM((ROWS, D), BF16),
+            pltpu.VMEM((16, 128), F32),
+            pltpu.VMEM((16, 128), F32),
+            pltpu.VMEM((3, ROWS, 256), BF16),
+            pltpu.VMEM((1, D), F32),
+            pltpu.VMEM((3, 128), BF16),
+            pltpu.VMEM((3, 2, 64), BF16),
+            pltpu.VMEM((2, 16), F32),
+            pltpu.VMEM((2, 2, 128), F32),
+            pltpu.VMEM((1, 16), F32),
+            pltpu.VMEM((1, 128), F32),
+            pltpu.VMEM((1, D), F32),
             pltpu.VMEM((CTX, D), BF16),
-            pltpu.VMEM((D, 64), BF16),
-            pltpu.VMEM((D, 64), BF16),
-            pltpu.VMEM((D, 32), BF16),
+            pltpu.VMEM((256, D), BF16),
             pltpu.VMEM((128, D), BF16),
             pltpu.VMEM((D, 512), BF16),
             pltpu.VMEM((NY, 4, 128), F32),
             pltpu.VMEM((NI, 4, 128), F32),
             pltpu.VMEM((4, 128), F32),
             pltpu.VMEM((NA, 4, 128), F32),
-            pltpu.VMEM((NY, 4, 128), F32),
-            pltpu.VMEM((NT, NY, 4, 128), F32),
-            pltpu.VMEM((NT + 2, ROWS, D), BF16),
-            pltpu.VMEM((NT + 2, ROWS, D), F32),
+            pltpu.VMEM((4, 128), F32),
+            pltpu.VMEM((NY * NT, 4, 128), F32),
+            pltpu.VMEM((NT, ROWS, D), BF16),
+            pltpu.VMEM((2, 1, D), F32),
+            pltpu.VMEM((2, 1, D), F32),
+            pltpu.VMEM((NT + 1, ROWS, D), F32),
             pltpu.VMEM((CTX, D), F32),
-            pltpu.VMEM(((NT + 2) * ROWS, D), BF16),
+            pltpu.VMEM(((NT + 1) * ROWS, D), BF16),
             pltpu.VMEM((128, D), BF16),
             pltpu.VMEM((CTX, 384), F32),
             pltpu.VMEM((2, 128), F32),
             pltpu.VMEM((NI, 2, 128), F32),
             pltpu.VMEM((2, 128), F32),
             pltpu.VMEM((NA, 2, 128), F32),
-            pltpu.VMEM((NI, 8, 128), F32),
-            pltpu.VMEM((NI, 8, 128), F32),
-            pltpu.VMEM((8, 128), F32),
-            pltpu.VMEM((NA, 8, 128), F32),
+            pltpu.VMEM((NI, 8, 128), BF16),
+            pltpu.VMEM((NI, 8, 128), BF16),
+            pltpu.VMEM((8, 128), BF16),
+            pltpu.VMEM((NA, 8, 128), BF16),
             pltpu.VMEM((NI, 8, 128), F32),
             pltpu.VMEM((NI, 1, 128), F32),
             pltpu.VMEM((NI, 8, 128), F32),
-            pltpu.VMEM((NI, 8, 128), F32),
-            pltpu.VMEM((NI, 8, 128), F32),
+            pltpu.VMEM((NI, 8, 128), BF16),
+            pltpu.VMEM((NI, 8, 128), BF16),
             pltpu.VMEM((NT, ROWS, D), BF16),
             pltpu.VMEM((NT, ROWS, D), BF16),
+            dma((12,)),
             dma((7,)),
             dma((4, NI)),
             dma((4, NI)),
@@ -574,8 +630,8 @@
             dma((3, NA)),
             dma((3, NT)),
             dma((3, NT)),
-            dma((NY,)),
-            dma((NY,)),
+            dma((NY * NT,)),
+            dma((NY * NT,)),
             dma((2,)),
             dma((2,)),
         ],
@@ -586,21 +642,21 @@
         latent,
         condition.reshape(16, 128),
         context_condition.reshape(16, 128),
-        modulation_weight.reshape(ROWS, 768),
+        modulation_weight.transpose(1, 0, 2),
         norm_gain.reshape(1, D),
         value_taps,
         map_taps,
         decay_rate,
         decay_jump,
-        skip_gain,
+        skip_gain.reshape(1, 16),
         group_gain.reshape(1, 128),
         post_gain.reshape(1, D),
         context,
         gate_weight,
         value_weight,
-        write_weight,
-        read_weight,
-        step_weight.reshape(D, 32),
+        write_weight.T,
+        read_weight.T,
+        step_weight.transpose(1, 2, 0).reshape(32, D),
         output_weight,
     )
 

time: 98.1 us -> 87.4 us (0.89)
  local copies, waits for them, and re-layouts: 8.67 us -> 1.47 us
  Pallas kernels: 89.1 us -> 85.7 us
    unnamed x3 -> x1, local copies, waits for them, and re-layouts: 5.39 us -> 1.47 us
    pallas_call x1, Pallas kernels: 89.1 us -> 85.7 us  [body(): pl.pallas_call(kernel, out_shape=jax.ShapeDtypeStruct((ROWS, D), BF16), i...]
    reshape x2 -> x0, local copies, waits for them, and re-layouts: 3.28 us -> none  [the longest x1 1.93 us: body(): step_weight.reshape(D, 32)]
where the time goes in v1:
time: 87.4 us; the launch traced here: 87.2 us
  Pallas kernels  85.7 us (98%)
  local copies, waits for them, and re-layouts  1.47 us (2%)
    pallas_call x1, Pallas kernels, body(): pl.pallas_call(kernel, out_shape=jax.ShapeDtypeStruct((ROWS, D), BF16), i...  85.7 us

profile of v1, /device:TPU:1, one launch (start us, length us, event | category | flops | bytes accessed | tf_op | source)
XLA Modules:
  0.0 87.2 jit_solution(6227003266449488724)
XLA Ops:
  0.0 85.7 %shard_map.181 = bf16[16,2048]{1,0:T(8,128)(2,1)} custom-call(bf16[16,2048]{1,0:T(8,128)(2,1)} %latent_h.1, f32[16,128]{1,0:T(8,128)} %bitcast.16, f32[16,128]{1,0:T(8,128)} %bitcast.17, bf16[3,16,256]{2,1,0:T(8,128)(2,1)} %bitcast.15, f32[1,2048]{1,0:T(1,128)} %bitcast.18, bf16[3,128]{1,0:T(4,128)(2,1)} %vtaps_h.1, bf16[3,2,64]{2,1,0:T(2,128)(2,1)} %mtaps_h.1, ...), custom_call_target="tpu_custom_call" | custom-call | tf_op jit(solution)/shard_map/pallas_call | solution.py:574
  85.7 1.5 %copy.21 = bf16[16,2048]{1,0:T(8,128)(2,1)} copy(bf16[16,2048]{1,0:T(8,128)(2,1)} %shard_map.181) | data formatting | bytes 131072

commit v2 on v1

--- a/solution.py
+++ b/solution.py
@@ -81,7 +81,6 @@
     wall,
     part,
     r1,
-    s1,
     r2,
     s2,
     r4,
@@ -118,6 +117,8 @@
     tp_rsem,
     plane_ssem,
     plane_rsem,
+    ring_ssem,
+    ring_rsem,
     halo_ssem,
     halo_rsem,
 ):
@@ -147,6 +148,8 @@
 
     following = at_range(lax.rem(s + 1, NS))
     preceding = at_range(lax.rem(s + NS - 1, NS))
+    next_block = {"za": lax.rem(a + 1, NA)}
+    last_block = {"za": lax.rem(a + NA - 1, NA)}
 
     def copy(src, dst, ssem, rsem, device):
         return pltpu.make_async_remote_copy(
@@ -156,42 +159,15 @@
     def exchange(n, me, peer, src_of, dst, ssem, rsem):
         def begin(k, carry):
             j = lax.rem(me + k, n)
-            copy(src_of(j), dst.at[me], ssem.at[k], rsem.at[me], peer(j)).start()
+            copy(src_of(j), dst.at[me], ssem, rsem, peer(j)).start()
             return carry
 
-        def arrive(k, carry):
-            j = lax.rem(me + n - k, n)
-            copy(src_of(j), dst.at[j], ssem.at[k], rsem.at[j], peer(j)).wait_recv()
-            return carry
-
-        def leave(k, carry):
-            j = lax.rem(me + k, n)
-            copy(src_of(j), dst.at[me], ssem.at[k], rsem.at[me], peer(j)).wait_send()
-            return carry
-
+        others = dst.at[pl.ds(0, n - 1)]
         return (
             lambda: lax.fori_loop(1, n, begin, 0),
-            lambda: lax.fori_loop(1, n, arrive, 0),
-            lambda: lax.fori_loop(1, n, leave, 0),
+            lambda: pltpu.make_async_copy(others, others, rsem).wait(),
+            lambda: pltpu.make_async_copy(others, others, ssem).wait(),
         )
-
-    barrier = pltpu.get_barrier_semaphore()
-
-    def tell(device):
-        pl.semaphore_signal(barrier, inc=1, device_id=device, device_id_type=MESH)
-
-    def tell_all(n, me, peer):
-        def one(k, carry):
-            tell(peer(lax.rem(me + k, n)))
-            return carry
-
-        lax.fori_loop(1, n, one, 0)
-
-    tell_all(NA, a, far)
-    tell_all(NI, i, near)
-    tell_all(NY * NT, g, plane)
-    tell(following)
-    tell(preceding)
 
     small = [
         pltpu.make_async_copy(src, dst, small_sem.at[n])
@@ -214,6 +190,25 @@
     ]
     for load in small:
         load.start()
+    barrier = pltpu.get_barrier_semaphore()
+
+    def tell(device):
+        pl.semaphore_signal(barrier, inc=1, device_id=device, device_id_type=MESH)
+
+    def tell_all(n, me, peer):
+        def one(k, carry):
+            tell(peer(lax.rem(me + k, n)))
+            return carry
+
+        lax.fori_loop(1, n, one, 0)
+
+    tell(next_block)
+    tell(last_block)
+    tell_all(NI, i, near)
+    tell_all(NY * NT, g, plane)
+    tell(following)
+    tell(preceding)
+
     loads = [
         pltpu.make_async_copy(gate_h, wall.at[:, pl.ds(0, 128)], load_sem.at[0]),
         pltpu.make_async_copy(value_h, wall.at[:, pl.ds(128, 128)], load_sem.at[1]),
@@ -244,20 +239,46 @@
     m1_start, m1_wait, m1_left = exchange(
         NI, i, near, lambda j: part.at[lax.rem(j, NY)], r1, near_ssem.at[0], near_rsem.at[0]
     )
-    m2_start, m2_wait, m2_left = exchange(NA, a, far, lambda j: s1, r2, far_ssem.at[0], far_rsem.at[0])
-    m3_start, m3_wait, m3_left = exchange(NY * NT, g, plane, lambda j: s2, r4, plane_ssem, plane_rsem)
+
+    def block(k):
+        return r2.at[lax.rem(a + k + NA, NA)]
+
+    def relay(k):
+        found = [copy(block(1 - k), block(1 - k), ring_ssem.at[k - 1], ring_rsem.at[k - 1], next_block)]
+        if k < NA // 2:
+            found.append(copy(block(k - 1), block(k - 1), ring_ssem.at[k + 3], ring_rsem.at[k + 3], last_block))
+        return found
+
+    def relay_start(k):
+        for c in relay(k):
+            c.start()
+
+    def relay_wait(k):
+        copy(block(-k), block(-k), ring_ssem.at[k - 1], ring_rsem.at[k - 1], next_block).wait_recv()
+        if k < NA // 2:
+            copy(block(k), block(k), ring_ssem.at[k + 3], ring_rsem.at[k + 3], last_block).wait_recv()
+
+    def relay_left():
+        for k in range(1, NA // 2 + 1):
+            for c in relay(k):
+                c.wait_send()
+
+    m3_start, m3_wait, m3_left = exchange(NY * NT, g, plane, lambda j: s2, r4, plane_ssem.at[0], plane_rsem.at[0])
     x_start, x_wait, x_left = exchange(NT, t, along_tp, lambda j: latent, xg, tp_ssem.at[0], tp_rsem.at[0])
 
-    pl.semaphore_wait(barrier, (NA - 1) + (NI - 1) + (NY * NT - 1) + 2)
+    pl.semaphore_wait(barrier, 2 + (NI - 1) + (NY * NT - 1) + 2)
 
     m1_start()
     r1[i] = part[y]
     x_start()
     xg[t] = latent[...]
 
+    m1_wait()
+    r2[a] = jnp.sum(r1[...], axis=0)
+    relay_start(1)
+
     for load in loads[:5]:
         load.wait()
-
     rest_v[160:256, :] = jnp.zeros((96, D), BF16)
 
     def join(k, carry):
@@ -266,11 +287,8 @@
         return carry
 
     lax.fori_loop(0, D // 256, join, 0)
-
-    m1_wait()
-    s1[...] = jnp.sum(r1[...], axis=0)
-    m2_start()
-    r2[a] = s1[...]
+    relay_wait(1)
+    relay_start(2)
 
     x_wait()
     hsend[0] = xg[NT - 1].astype(F32)[15:16, :]
@@ -289,6 +307,9 @@
         return carry
 
     lax.fori_loop(0, NT, norm_latent, 0)
+    relay_wait(2)
+    relay_start(3)
+
     up.wait_recv()
     down.wait_recv()
     xn[NT] = jnp.concatenate([normed(hrecv[0]), normed(hrecv[1]), jnp.zeros((14, D), F32)], axis=0)
@@ -299,9 +320,11 @@
         cn[at, :] = normed(context_v[at, :].astype(F32))
         return carry
 
-    lax.fori_loop(0, CTX // 16, norm_context, 0)
-
-    m2_wait()
+    lax.fori_loop(0, CTX // 32, norm_context, 0)
+    relay_wait(3)
+    relay_start(4)
+    lax.fori_loop(CTX // 32, CTX // 16, norm_context, 0)
+    relay_wait(4)
     s2[...] = jnp.sum(r2[...], axis=0)
     m3_start()
     r4[g] = s2[...]
@@ -429,7 +452,7 @@
 
     l1_wait()
     l2send[...] = jnp.sum(rl1[...], axis=0)
-    l2_start, l2_wait, l2_left = exchange(NA, a, far, lambda j: l2send, rl2, far_ssem.at[1], far_rsem.at[1])
+    l2_start, l2_wait, l2_left = exchange(NA, a, far, lambda j: l2send, rl2, far_ssem.at[0], far_rsem.at[0])
     l2_start()
     rl2[a] = l2send[...]
 
@@ -448,7 +471,7 @@
         0, NI, fold, (jnp.zeros((8, 128), F32), jnp.ones((1, 128), F32))
     )
     bt[...] = block_state.astype(BF16)
-    s2_start, s2_wait, s2_left = exchange(NA, a, far, lambda j: bt, rs2, far_ssem.at[2], far_rsem.at[2])
+    s2_start, s2_wait, s2_left = exchange(NA, a, far, lambda j: bt, rs2, far_ssem.at[1], far_rsem.at[1])
     s2_start()
     rs2[a] = bt[...]
 
@@ -491,7 +514,7 @@
     for d in range(2):
         cst[8 * d : 8 * d + 8] = context_state[d].reshape(8, 8, 128)
 
-    for left in (m1_left, m2_left, m3_left, x_left, l1_left, s1_left, l2_left, s2_left):
+    for left in (m1_left, relay_left, m3_left, x_left, l1_left, s1_left, l2_left, s2_left):
         left()
     up.wait_send()
     down.wait_send()
@@ -530,7 +553,7 @@
         oo[:, :, at] = (
             jnp.dot(gated, outw_v[:, at], preferred_element_type=F32).astype(BF16).reshape(NT, ROWS, 512)
         )
-    o_start, o_wait, o_left = exchange(NT, t, along_tp, lambda j: oo.at[j], ro, tp_ssem.at[2], tp_rsem.at[2])
+    o_start, o_wait, o_left = exchange(NT, t, along_tp, lambda j: oo.at[j], ro, tp_ssem.at[1], tp_rsem.at[1])
     o_start()
     ro[t] = oo[t]
     gate0 = vector(0, 2)
@@ -573,7 +596,7 @@
     dma = pltpu.SemaphoreType.DMA
     return pl.pallas_call(
         kernel,
-        out_shape=jax.ShapeDtypeStruct((ROWS, D), BF16),
+        out_shape=pltpu.VMEM((ROWS, D), BF16),
         in_specs=[hbm] * 19,
         out_specs=vmem,
         scratch_shapes=[
@@ -595,7 +618,6 @@
             pltpu.VMEM((D, 512), BF16),
             pltpu.VMEM((NY, 4, 128), F32),
             pltpu.VMEM((NI, 4, 128), F32),
-            pltpu.VMEM((4, 128), F32),
             pltpu.VMEM((NA, 4, 128), F32),
             pltpu.VMEM((4, 128), F32),
             pltpu.VMEM((NY * NT, 4, 128), F32),
@@ -624,14 +646,16 @@
             pltpu.VMEM((NT, ROWS, D), BF16),
             dma((12,)),
             dma((7,)),
-            dma((4, NI)),
-            dma((4, NI)),
-            dma((3, NA)),
-            dma((3, NA)),
-            dma((3, NT)),
-            dma((3, NT)),
-            dma((NY * NT,)),
-            dma((NY * NT,)),
+            dma((4,)),
+            dma((4,)),
+            dma((2,)),
+            dma((2,)),
+            dma((2,)),
+            dma((2,)),
+            dma((1,)),
+            dma((1,)),
+            dma((NA - 1,)),
+            dma((NA - 1,)),
             dma((2,)),
             dma((2,)),
         ],

time: 87.4 us -> 83.7 us (0.958)
  Pallas kernels: 85.7 us -> 83 us
    pallas_call x1, Pallas kernels: 85.7 us -> 83 us  [body(): pl.pallas_call(kernel, out_shape=pltpu.VMEM((ROWS, D), BF16), in_specs=[h...]
where the time goes in v2:
time: 83.7 us; the launch traced here: 83.6 us
  Pallas kernels  83 us (99%)
    pallas_call x1, Pallas kernels, body(): pl.pallas_call(kernel, out_shape=pltpu.VMEM((ROWS, D), BF16), in_specs=[h...  83 us

profile of v2, /device:TPU:1, one launch (start us, length us, event | category | flops | bytes accessed | tf_op | source)
XLA Modules:
  0.0 83.6 jit_solution(6847743995576563569)
XLA Ops:
  0.0 83.0 %shard_map.181 = bf16[16,2048]{1,0:T(8,128)(2,1)S(1)} custom-call(bf16[16,2048]{1,0:T(8,128)(2,1)} %latent_h.1, f32[16,128]{1,0:T(8,128)} %bitcast.16, f32[16,128]{1,0:T(8,128)} %bitcast.17, bf16[3,16,256]{2,1,0:T(8,128)(2,1)} %bitcast.15, f32[1,2048]{1,0:T(1,128)} %bitcast.18, bf16[3,128]{1,0:T(4,128)(2,1)} %vtaps_h.1, bf16[3,2,64]{2,1,0:T(2,128)(2,1)} %mtaps_h.1, ...), custom_call_target="tpu_custom_call" | custom-call | tf_op jit(solution)/shard_map/pallas_call | solution.py:597
  83.0 0.6 copy.21
